TPU v7x, 32 devices: a whole 2x2x4 slice. The times are simulated.
32 devices in a mesh: kv: 4 (over y, x), tp: 8 (over z, core).
Axes of the slice: x: 2, y: 2, z: 4, core: 2. Of those that a mesh axis runs over, the one named last changes fastest.
Arguments:
- residual: bfloat16 [128, 4096], P(None, ('kv', 'tp')), may hold values from -20 to 20
- mixer_gain: float32 [4096], P('kv'), may hold values from 0.1 to 1.9
- w_query: bfloat16 [4096, 4096], P('kv', 'tp'), may hold values from -0.09375 to 0.09375
- w_forget: bfloat16 [4096, 4096], P('kv', 'tp'), may hold values from -0.09375 to 0.09375
- w_input: bfloat16 [4096, 4096], P('kv', 'tp'), may hold values from -0.09375 to 0.09375
- w_outgate: bfloat16 [4096, 4096], P('kv', 'tp'), may hold values from -0.09375 to 0.09375
- lower_bound: float32 [4096], P('tp'), may hold values from 0.3 to 0.97
- state: float32 [128, 32, 128, 128], P('kv', 'tp'), may hold values from -6 to 6
- head_gain: float32 [128], replicated, may hold values from 0.1 to 1.9
- w_mix_out: bfloat16 [4096, 4096], P('tp', 'kv'), may hold values from -0.09375 to 0.09375
- ffn_gain: float32 [4096], P('kv'), may hold values from 0.1 to 1.9
- w_gate: bfloat16 [4096, 10752], P('kv', 'tp'), may hold values from -0.09375 to 0.09375
- w_up: bfloat16 [4096, 10752], P('kv', 'tp'), may hold values from -0.09375 to 0.09375
- w_down: bfloat16 [10752, 4096], P('tp', 'kv'), may hold values from -0.0625 to 0.0625
Outputs:
- layer_out: bfloat16 [128, 4096], P(None, ('kv', 'tp'))
- new_state: float32 [128, 32, 128, 128], P('kv', 'tp')
All inputs are finite; a program needn't handle non-finite values.
Results may differ from a plain program's by a relative error of at most 0.015.
Values may be sent and summed in bfloat16 or wider, within the bound.
No kernel may reach another device: no remote copies, remote signals or barrier semaphores. Data moves between devices by JAX's collectives and lax.ppermute only.
A program may use at most 64 MiB of HBM per device.

v0:
```python
import jax
import jax.numpy as jnp
from jax import lax
from jax.sharding import PartitionSpec as P

D = 4096
DK = 128
DV = 128
EPS = 1e-06


def project_row(weight, piece):
    return jnp.dot(piece, weight, preferred_element_type=jnp.float32)


def channel_mix(rows_in, ffn_gain, w_gate, w_up, w_down):
    rows_float = rows_in.astype(jnp.float32)
    squares = jnp.sum(rows_float * rows_float, axis=1)
    scaled = (rows_float * ffn_gain).astype(jnp.bfloat16)
    gate = jnp.dot(scaled, w_gate, preferred_element_type=jnp.float32)
    upper = jnp.dot(scaled, w_up, preferred_element_type=jnp.float32)
    whole_total = lax.psum(squares, "kv")
    gate, upper = (
        lax.psum(gate.astype(jnp.bfloat16), "kv").astype(jnp.float32),
        lax.psum(upper.astype(jnp.bfloat16), "kv").astype(jnp.float32),
    )
    inverse = lax.rsqrt(whole_total / D + EPS)[:, None]
    hidden = (jax.nn.silu(gate * inverse) * (upper * inverse)).astype(jnp.bfloat16)
    terms = jnp.dot(hidden, w_down, preferred_element_type=jnp.float32)
    summed = lax.psum_scatter(
        terms.astype(jnp.bfloat16), "tp", scatter_dimension=1, tiled=True
    ).astype(jnp.float32)
    width = summed.shape[1]
    own = lax.dynamic_slice_in_dim(rows_float, lax.axis_index("tp") * width, width, 1)
    return (own + summed).astype(jnp.bfloat16)


def body(
    residual,
    mixer_gain,
    w_query,
    w_forget,
    w_input,
    w_outgate,
    lower_bound,
    state,
    head_gain,
    w_mix_out,
    ffn_gain,
    w_gate,
    w_up,
    w_down,
):
    local_seqs, local_heads = (state.shape[0], state.shape[1])
    rows = lax.all_gather(residual, "tp", axis=1, tiled=True)
    rows_float = rows.astype(jnp.float32)
    squares = jnp.sum(rows_float * rows_float, axis=1)
    scaled = (rows_float * mixer_gain).astype(jnp.bfloat16)
    part_query = jnp.dot(scaled, w_query, preferred_element_type=jnp.float32)
    part_forget = jnp.dot(scaled, w_forget, preferred_element_type=jnp.float32)
    part_value = jnp.dot(scaled, w_input, preferred_element_type=jnp.float32)
    part_gate = jnp.dot(scaled, w_outgate, preferred_element_type=jnp.float32)
    whole_total = lax.psum(squares, "kv")
    total = lax.dynamic_slice_in_dim(whole_total, lax.axis_index("kv") * local_seqs, local_seqs)
    part_query, part_forget, part_value, part_gate = (
        lax.psum_scatter(part_query, "kv", scatter_dimension=0, tiled=True),
        lax.psum_scatter(part_forget, "kv", scatter_dimension=0, tiled=True),
        lax.psum_scatter(part_value, "kv", scatter_dimension=0, tiled=True),
        lax.psum_scatter(part_gate, "kv", scatter_dimension=0, tiled=True),
    )
    inverse = lax.rsqrt(total / D + EPS)[:, None]
    bound = lower_bound.reshape(local_heads, DK)
    forget_raw = (part_forget * inverse).reshape(local_seqs, local_heads, DK)
    forget = bound + (1.0 - bound) * jax.nn.sigmoid(forget_raw)
    keyvec = (1.0 - bound) * jax.nn.sigmoid(-forget_raw)
    query = jax.nn.silu((part_query * inverse).reshape(local_seqs, local_heads, DK))
    values = (part_value * inverse).reshape(local_seqs, local_heads, DV)
    updated = forget[..., None] * state + keyvec[..., None] * values[:, :, None, :]
    head_out = jnp.einsum("shc,shce->she", query, updated, precision=lax.Precision.HIGHEST)
    inv_head = lax.rsqrt(jnp.mean(head_out * head_out, axis=2, keepdims=True) + EPS)
    out_gate = jax.nn.silu((part_gate * inverse).reshape(local_seqs, local_heads, DV))
    normed = (
        (head_out * inv_head * head_gain * out_gate)
        .reshape(local_seqs, local_heads * DV)
        .astype(jnp.bfloat16)
    )
    terms = project_row(w_mix_out, lax.all_gather(normed, "kv", axis=0, tiled=True))
    mixed = lax.psum(terms, "tp")
    after_mix = (rows_float + mixed).astype(jnp.bfloat16)
    layer_out = channel_mix(after_mix, ffn_gain, w_gate, w_up, w_down)
    return (layer_out, updated)


def solution(mesh):
    in_specs = (
        P(None, ("kv", "tp")),
        P("kv"),
        P("kv", "tp"),
        P("kv", "tp"),
        P("kv", "tp"),
        P("kv", "tp"),
        P("tp"),
        P("kv", "tp", None, None),
        P(),
        P("tp", "kv"),
        P("kv"),
        P("kv", "tp"),
        P("kv", "tp"),
        P("tp", "kv"),
    )
    out_specs = (P(None, ("kv", "tp")), P("kv", "tp", None, None))
    return jax.shard_map(body, mesh=mesh, in_specs=in_specs, out_specs=out_specs, check_vma=False)
```

profile of v0, /device:TPU:0, one launch (start us, length us, event | category | flops | bytes accessed | tf_op | source)
XLA Modules:
  0.0 312.9 jit_solution(12020792351462122957)
XLA Ops:
  7.2 0.0 copy-start
  7.2 0.0 reduce-scatter.10.cloned.1.call-start
  7.2 15.1 %all_gather.6 = bf16[128,1024]{1,0:T(8,128)(2,1)S(1)} all-gather(bf16[128,128]{1,0:T(8,128)(2,1)} %param.14), channel_id=1, replica_groups=mesh['kv'=4,'tp'=8] {'tp'}, dimensions={1}, use_global_device_ids=true | all-gather | bytes 294912 | tf_op jit(solution)/shard_map/all_gather | solution.py:55
  22.4 2.3 fusion.10
  24.6 0.0 reduce-scatter.10.cloned.1.call-update
  24.7 0.0 reduce-scatter.12.cloned.1.call-start
  24.7 2.2 fusion.8
  27.0 0.0 reduce-scatter.12.cloned.1.call-update
  27.0 0.0 reduce-scatter.14.cloned.1.call-start
  27.0 2.3 fusion.6
  29.3 0.0 reduce-scatter.14.cloned.1.call-update
  29.3 0.0 reduce-scatter.8.cloned.1.call-start
  29.4 2.3 fusion.12
  31.6 0.0 reduce-scatter.8.cloned.1.call-update
  31.7 0.0 all-reduce.4.cloned.1.call-start
  31.7 0.1 fusion.1
  31.8 9.9 %psum.35 = f32[128]{0:T(128)S(1)} all-reduce(f32[128]{0:T(128)S(1)} %fusion.1), channel_id=1, replica_groups=mesh['kv'=4,'tp'=8] {'kv'}, use_global_device_ids=true, to_apply=%region_2.0 | all-reduce | flops 128 | bytes 1024 | tf_op jit(solution)/shard_map/psum | solution.py:63
  41.8 0.1 add_rsqrt_fusion.2
  41.8 0.7 broadcast_subtract_fusion
  42.5 6.5 %reduce-scatter.10.cloned.1.call-done = f32[32,512]{1,0:T(8,128)} async-done(((f32[128,512]{1,0:T(8,128)}), f32[32,512]{1,0:T(8,128)}) %reduce-scatter.10.cloned.1.call-update) | async-done | bytes 65552 | tf_op jit(solution)/shard_map/reduce_scatter | solution.py:67
  49.0 27.1 %reduce-scatter.12.cloned.1.call-done = f32[32,512]{1,0:T(8,128)} async-done(((f32[128,512]{1,0:T(8,128)}), f32[32,512]{1,0:T(8,128)}) %reduce-scatter.12.cloned.1.call-update) | async-done | bytes 65552 | tf_op jit(solution)/shard_map/reduce_scatter | solution.py:68
  76.1 27.2 %reduce-scatter.14.cloned.1.call-done = f32[32,512]{1,0:T(8,128)} async-done(((f32[128,512]{1,0:T(8,128)}), f32[32,512]{1,0:T(8,128)}) %reduce-scatter.14.cloned.1.call-update) | async-done | bytes 65552 | tf_op jit(solution)/shard_map/reduce_scatter | solution.py:69
  103.3 27.0 %reduce-scatter.8.cloned.1.call-done = f32[32,512]{1,0:T(8,128)} async-done(((f32[128,512]{1,0:T(8,128)}), f32[32,512]{1,0:T(8,128)}) %reduce-scatter.8.cloned.1.call-update) | async-done | bytes 65552 | tf_op jit(solution)/shard_map/reduce_scatter | solution.py:66
  130.3 1.0 add_divide_fusion.1
  131.6 8.2 %multiply_add_fusion = f32[32,4,128,128]{3,2,1,0:T(8,128)S(1)} fusion(f32[32,4,128,128]{3,2,1,0:T(8,128)} %param.21, f32[32,4,128]{2,1,0:T(4,128)S(1)} %mul.164, f32[32,4,128]{2,1,0:T(4,128)S(1)} %bitcast.35, f32[32,4,128]{2,1,0:T(4,128)S(1)} %bitcast.34), kind=kLoop, calls=%fused_computation | loop fusion | flops 6291456 | bytes 16973824 | tf_op jit(solution)/shard_map/add | solution.py:78
  139.8 0.0 copy-start.1
  139.9 3.4 %copy-done.1 = f32[32,4,128,128]{3,2,1,0:T(8,128)} copy-done((f32[32,4,128,128]{3,2,1,0:T(8,128)}, f32[32,4,128,128]{3,2,1,0:T(8,128)S(1)}, u32[]{:S(2)}) %copy-start.1) | copy-done | bytes 8388632
  143.2 7.2 %fusion.18 = f32[32,4,1,128]{3,2,1,0:T(1,128)S(1)} fusion(f32[32,4,128,1]{2,3,1,0:T(1,128)S(1)} %bitcast.33, f32[32,4,128,128]{3,2,1,0:T(8,128)S(1)} %multiply_add_fusion), kind=kOutput, calls=%fused_computation.39 | convolution fusion | flops 25165824 | bytes 8519680 | tf_op jit(solution)/shard_map/shc,shce->she/dot_general | solution.py:79
  150.5 0.1 multiply_reduce_fusion.1
  150.6 0.1 fusion.15
  150.8 8.5 %all_gather.7 = bf16[128,512]{1,0:T(8,128)(2,1)S(1)} all-gather(bf16[32,512]{1,0:T(8,128)(2,1)S(1)} %bitcast.38), channel_id=1, replica_groups=mesh['kv'=4,'tp'=8] {'kv'}, dimensions={0}, use_global_device_ids=true | all-gather | bytes 163840 | tf_op jit(solution)/shard_map/all_gather | solution.py:87
  159.2 1.1 fusion.19
  160.4 0.0 all-reduce.4.cloned.1.call-update
  160.4 0.0 all-reduce.6.cloned.1.call-start
  160.4 56.7 %all-reduce.4.cloned.1.call-done = f32[128,1024]{1,0:T(8,128)} async-done(((f32[128,1024]{1,0:T(8,128)}), f32[128,1024]{1,0:T(8,128)}) %all-reduce.4.cloned.1.call-update) | async-done | bytes 524304 | tf_op jit(solution)/shard_map/psum | solution.py:88
  217.1 1.2 multiply_reduce_fusion
  218.3 1.6 convolution_convert_fusion
  219.9 3.4 %convolution_convert_fusion.1 = bf16[128,1344]{0,1:T(8,128)(2,1)} fusion(bf16[1024,1344]{0,1:T(8,128)(2,1)} %param.25, f32[128,1024]{1,0:T(8,128)S(1)} %get-tuple-element.5, f32[1024]{0:T(1024)S(1)} %copy-done.3), kind=kOutput, calls=%fused_computation.2 | convolution fusion | flops 352755712 | bytes 3624960 | tf_op jit(solution)/shard_map/dot_general | solution.py:20
  223.3 0.0 all-reduce.6.cloned.1.call-update
  223.4 0.0 reduce-scatter.16.cloned.1.call-start
  223.4 10.2 %psum.38 = f32[128]{0:T(128)S(1)} all-reduce(f32[128]{0:T(128)S(1)} %get-tuple-element.4), channel_id=1, replica_groups=mesh['kv'=4,'tp'=8] {'kv'}, use_global_device_ids=true, to_apply=%region_10.11 | all-reduce | flops 128 | bytes 1024 | tf_op jit(solution)/shard_map/psum | solution.py:22
  233.6 36.4 %all-reduce.6.cloned.1.call-done = (bf16[128,1344]{0,1:T(8,128)(2,1)}, bf16[128,1344]{0,1:T(8,128)(2,1)}) async-done(((bf16[128,1344]{0,1:T(8,128)(2,1)}, bf16[128,1344]{0,1:T(8,128)(2,1)}), (bf16[128,1344]{0,1:T(8,128)(2,1)}, bf16[128,1344]{0,1:T(8,128)(2,1)})) %all-reduce.6.cloned.1.call-update) | async-done | bytes 688144 | tf_op jit(solution)/shard_map/psum | solution.py:25
  270.0 2.8 convolution_convert_fusion.2
  272.7 0.8 copy.18
  273.6 0.0 reduce-scatter.16.cloned.1.call-update
  273.6 31.0 %reduce-scatter.16.cloned.1.call-done = bf16[128,128]{1,0:T(8,128)(2,1)} async-done(((bf16[1024,128]{1,0:T(8,128)(2,1)}), bf16[128,128]{1,0:T(8,128)(2,1)}) %reduce-scatter.16.cloned.1.call-update) | async-done | bytes 32784
  304.5 0.9 copy.19
  305.4 0.6 add_convert_fusion
  (21 shorter events, 0.2 us)
Async XLA Ops:
  7.2 211.1 %copy-start = (bf16[1024,1344]{0,1:T(8,128)(2,1)S(1)}, bf16[1024,1344]{0,1:T(8,128)(2,1)}, u32[]{:S(2)}) copy-start(bf16[1024,1344]{0,1:T(8,128)(2,1)} %param.26) | copy-start | bytes 8257540
  7.2 124.4 %copy-start.4 = (f32[512]{0:T(512)S(1)}, f32[512]{0:T(512)}, u32[]{:S(2)}) copy-start(f32[512]{0:T(512)} %param.20) | copy-start | bytes 6148
  7.2 41.8 %reduce-scatter.10.cloned.1.call-start = ((), (), s32[]{:S(2)}) async-start(), calls=%async_computation.6 | async-start | bytes 327680 | tf_op jit(solution)/shard_map/reduce_scatter | solution.py:67
  24.7 51.5 %reduce-scatter.12.cloned.1.call-start = ((), (), s32[]{:S(2)}) async-start(), calls=%async_computation.7 | async-start | bytes 327680 | tf_op jit(solution)/shard_map/reduce_scatter | solution.py:68
  27.0 76.3 %reduce-scatter.14.cloned.1.call-start = ((), (), s32[]{:S(2)}) async-start(), calls=%async_computation.8 | async-start | bytes 327680 | tf_op jit(solution)/shard_map/reduce_scatter | solution.py:69
  29.3 101.0 %reduce-scatter.8.cloned.1.call-start = ((), (), s32[]{:S(2)}) async-start(), calls=%async_computation.5 | async-start | bytes 327680 | tf_op jit(solution)/shard_map/reduce_scatter | solution.py:66
  31.7 185.4 %all-reduce.4.cloned.1.call-start = ((), (), s32[]{:S(2)}) async-start(), calls=%async_computation.9 | async-start | bytes 1048576 | tf_op jit(solution)/shard_map/psum | solution.py:88
  139.8 3.4 %copy-start.1 = (f32[32,4,128,128]{3,2,1,0:T(8,128)}, f32[32,4,128,128]{3,2,1,0:T(8,128)S(1)}, u32[]{:S(2)}) copy-start(f32[32,4,128,128]{3,2,1,0:T(8,128)S(1)} %multiply_add_fusion) | copy-start | bytes 25165828
  139.8 10.8 %copy-start.5 = (f32[128]{0:T(128)S(1)}, f32[128]{0:T(128)}, u32[]{:S(2)}) copy-start(f32[128]{0:T(128)} %param.22) | copy-start | bytes 1540
  139.9 19.4 %copy-start.2 = (bf16[512,1024]{1,0:T(8,128)(2,1)S(1)}, bf16[512,1024]{1,0:T(8,128)(2,1)}, u32[]{:S(2)}) copy-start(bf16[512,1024]{1,0:T(8,128)(2,1)} %param.23) | copy-start | bytes 3145732
  139.9 78.4 %copy-start.3 = (f32[1024]{0:T(1024)S(1)}, f32[1024]{0:T(1024)}, u32[]{:S(2)}) copy-start(f32[1024]{0:T(1024)} %param.24) | copy-start | bytes 12292
  160.4 109.6 %all-reduce.6.cloned.1.call-start = ((), (), s32[]{:S(2)}) async-start(), calls=%async_computation.11 | async-start | bytes 1376256 | tf_op jit(solution)/shard_map/psum | solution.py:25
  223.4 81.2 %reduce-scatter.16.cloned.1.call-start = ((), (), s32[]{:S(2)}) async-start(), calls=%async_computation.10 | async-start | bytes 294912
Sparse Core Ops, SparseCore 0:
  24.8 24.1 reduce-scatter.9
  51.7 24.3 reduce-scatter.11
  78.9 24.3 reduce-scatter.13
  105.9 24.3 reduce-scatter.7
  160.5 56.5 all-reduce.3
  223.5 46.4 all-reduce.5
  273.7 30.7 reduce-scatter.15
where the time goes:
time: 314 us; the launch traced here: 313 us
  waiting for transfers between devices  212 us (68%)
  blocking collectives  43.7 us (14%)
  matrix products  25.2 us (8%)
  between operations  14.3 us (5%)
  other arithmetic  12.3 us (4%)
  local copies, waits for them, and re-layouts  5.22 us (2%)
    psum x1, waiting for transfers between devices, body(): mixed = lax.psum(terms, 'tp')  56.7 us
    psum x1, waiting for transfers between devices, channel_mix(): lax.psum(upper.astype(jnp.bfloat16), 'kv').astype(jnp.float32)  36.4 us
    unnamed x8, waiting for transfers between devices  31.1 us
    reduce_scatter x1, waiting for transfers between devices, body(): lax.psum_scatter(part_gate, 'kv', scatter_dimension=0, tiled=True)  27.2 us
    reduce_scatter x1, waiting for transfers between devices, body(): lax.psum_scatter(part_value, 'kv', scatter_dimension=0, tiled=True)  27.1 us
    reduce_scatter x1, waiting for transfers between devices, body(): lax.psum_scatter(part_query, 'kv', scatter_dimension=0, tiled=True)  27 us
    all_gather x1, blocking collectives, body(): rows = lax.all_gather(residual, 'tp', axis=1, tiled=True)  15.1 us
    psum x1, blocking collectives, channel_mix(): whole_total = lax.psum(squares, 'kv')  10.2 us
  transfers between devices with their start and end apart: 7, of which 7 were waited for; matrix products, arithmetic and copies ran while one was open for 2% of the time, Pallas kernels for 0%

commit v1 on v0

--- a/solution.py
+++ b/solution.py
@@ -85,7 +85,11 @@
         .astype(jnp.bfloat16)
     )
     terms = project_row(w_mix_out, lax.all_gather(normed, "kv", axis=0, tiled=True))
-    mixed = lax.psum(terms, "tp")
+    size = lax.axis_size("tp")
+    mixed, far = (terms, 1)
+    while far < size:
+        mixed = mixed + lax.ppermute(mixed, "tp", [(i, i ^ far) for i in range(size)])
+        far = 2 * far
     after_mix = (rows_float + mixed).astype(jnp.bfloat16)
     layer_out = channel_mix(after_mix, ffn_gain, w_gate, w_up, w_down)
     return (layer_out, updated)

time: 314 us -> 292 us (0.930)
  waiting for transfers between devices: 212 us -> 194 us
  starting transfers between devices: 0.29 us -> 4.34 us
  local copies, waits for them, and re-layouts: 5.22 us -> 1.87 us
    psum x1 -> x0, waiting for transfers between devices: 56.7 us -> none  [body(): mixed = lax.psum(terms, 'tp')]
    ppermute x0 -> x3, waiting for transfers between devices: none -> 37.2 us  [body(): lax.ppermute(mixed, 'tp', [(i, i ^ far) for i in range(size)])]
    ppermute x0 -> x3, starting transfers between devices: none -> 4.09 us  [body(): lax.ppermute(mixed, 'tp', [(i, i ^ far) for i in range(size)])]
    unnamed x17 -> x19, local copies, waits for them, and re-layouts: 5.09 us -> 1.75 us
    unnamed x8 -> x7, waiting for transfers between devices: 31.1 us -> 31.1 us
  transfers between devices with their start and end apart: 7 -> 9, of which waited for: 7 -> 9; matrix products, arithmetic and copies ran while one was open for 2% -> 3% of each run, Pallas kernels for 0% -> 0%
where the time goes in v1:
time: 292 us
  waiting for transfers between devices  194 us (66%)
  blocking collectives  42.6 us (15%)
  matrix products  22.6 us (8%)
  between operations  14.4 us (5%)
  other arithmetic  11.4 us (4%)
  starting transfers between devices  4.34 us (1%)
    psum x1, waiting for transfers between devices, channel_mix(): lax.psum(upper.astype(jnp.bfloat16), 'kv').astype(jnp.float32)  38.4 us
    ppermute x3, waiting for transfers between devices, body(): lax.ppermute(mixed, 'tp', [(i, i ^ far) for i in range(size)])  37.2 us
    unnamed x7, waiting for transfers between devices  31.1 us
    reduce_scatter x1, waiting for transfers between devices, body(): lax.psum_scatter(part_gate, 'kv', scatter_dimension=0, tiled=True)  27.2 us
    reduce_scatter x1, waiting for transfers between devices, body(): lax.psum_scatter(part_value, 'kv', scatter_dimension=0, tiled=True)  27.1 us
    reduce_scatter x1, waiting for transfers between devices, body(): lax.psum_scatter(part_query, 'kv', scatter_dimension=0, tiled=True)  27 us
    all_gather x1, blocking collectives, body(): rows = lax.all_gather(residual, 'tp', axis=1, tiled=True)  15.1 us
    psum x1, blocking collectives, body(): whole_total = lax.psum(squares, 'kv')  9.9 us
  transfers between devices with their start and end apart: 9, of which 9 were waited for; matrix products, arithmetic and copies ran while one was open for 3% of the time, Pallas kernels for 0%

profile of v1, /device:TPU:0, one launch (start us, length us, event | category | flops | bytes accessed | tf_op | source)
XLA Modules:
  0.0 291.6 jit_solution(11257893826951274100)
XLA Ops:
  7.2 0.0 reduce-scatter.10.cloned.1.call-start
  7.2 15.1 %all_gather.6 = bf16[128,1024]{1,0:T(8,128)(2,1)S(1)} all-gather(bf16[128,128]{1,0:T(8,128)(2,1)} %param.14), channel_id=1, replica_groups=mesh['kv'=4,'tp'=8] {'tp'}, dimensions={1}, use_global_device_ids=true | all-gather | bytes 294912 | tf_op jit(solution)/shard_map/all_gather | solution.py:55
  22.4 2.3 fusion.10
  24.6 0.0 reduce-scatter.10.cloned.1.call-update
  24.7 0.0 reduce-scatter.12.cloned.1.call-start
  24.7 2.2 fusion.8
  27.0 0.0 reduce-scatter.12.cloned.1.call-update
  27.0 0.0 reduce-scatter.14.cloned.1.call-start
  27.0 2.3 fusion.6
  29.3 0.0 reduce-scatter.14.cloned.1.call-update
  29.3 0.0 reduce-scatter.8.cloned.1.call-start
  29.4 2.2 fusion.12
  31.6 0.0 all-reduce.3.cloned.1.call-start
  31.7 0.1 fusion.1
  31.8 9.9 %psum.28 = f32[128]{0:T(128)S(1)} all-reduce(f32[128]{0:T(128)S(1)} %fusion.1), channel_id=1, replica_groups=mesh['kv'=4,'tp'=8] {'kv'}, use_global_device_ids=true, to_apply=%region_2.0 | all-reduce | flops 128 | bytes 1024 | tf_op jit(solution)/shard_map/psum | solution.py:63
  41.7 0.1 add_rsqrt_fusion.2
  41.8 0.7 broadcast_subtract_fusion
  42.5 6.5 %reduce-scatter.10.cloned.1.call-done = f32[32,512]{1,0:T(8,128)} async-done(((f32[128,512]{1,0:T(8,128)}), f32[32,512]{1,0:T(8,128)}) %reduce-scatter.10.cloned.1.call-update) | async-done | bytes 65552 | tf_op jit(solution)/shard_map/reduce_scatter | solution.py:67
  49.0 27.1 %reduce-scatter.12.cloned.1.call-done = f32[32,512]{1,0:T(8,128)} async-done(((f32[128,512]{1,0:T(8,128)}), f32[32,512]{1,0:T(8,128)}) %reduce-scatter.12.cloned.1.call-update) | async-done | bytes 65552 | tf_op jit(solution)/shard_map/reduce_scatter | solution.py:68
  76.1 27.2 %reduce-scatter.14.cloned.1.call-done = f32[32,512]{1,0:T(8,128)} async-done(((f32[128,512]{1,0:T(8,128)}), f32[32,512]{1,0:T(8,128)}) %reduce-scatter.14.cloned.1.call-update) | async-done | bytes 65552 | tf_op jit(solution)/shard_map/reduce_scatter | solution.py:69
  103.3 27.0 %reduce-scatter.8.cloned.1.call-done = f32[32,512]{1,0:T(8,128)} async-done(((f32[128,512]{1,0:T(8,128)}), f32[32,512]{1,0:T(8,128)}) %reduce-scatter.8.cloned.1.call-update) | async-done | bytes 65552 | tf_op jit(solution)/shard_map/reduce_scatter | solution.py:66
  130.3 1.0 add_divide_fusion.1
  131.6 8.2 %multiply_add_fusion = f32[32,4,128,128]{3,2,1,0:T(8,128)S(1)} fusion(f32[32,4,128,128]{3,2,1,0:T(8,128)} %param.21, f32[32,4,128]{2,1,0:T(4,128)S(1)} %mul.164, f32[32,4,128]{2,1,0:T(4,128)S(1)} %bitcast.35, f32[32,4,128]{2,1,0:T(4,128)S(1)} %bitcast.34), kind=kLoop, calls=%fused_computation | loop fusion | flops 6291456 | bytes 16973824 | tf_op jit(solution)/shard_map/add | solution.py:78
  139.9 7.2 %fusion.18 = f32[32,4,1,128]{3,2,1,0:T(1,128)S(1)} fusion(f32[32,4,128,1]{2,3,1,0:T(1,128)S(1)} %bitcast.33, f32[32,4,128,128]{3,2,1,0:T(8,128)S(1)} %multiply_add_fusion), kind=kOutput, calls=%fused_computation.39 | convolution fusion | flops 25165824 | bytes 8519680 | tf_op jit(solution)/shard_map/shc,shce->she/dot_general | solution.py:79
  147.1 0.1 multiply_reduce_fusion.1
  147.3 0.1 fusion.15
  147.4 8.5 %all_gather.7 = bf16[128,512]{1,0:T(8,128)(2,1)S(1)} all-gather(bf16[32,512]{1,0:T(8,128)(2,1)S(1)} %bitcast.38), channel_id=1, replica_groups=mesh['kv'=4,'tp'=8] {'kv'}, dimensions={0}, use_global_device_ids=true | all-gather | bytes 163840 | tf_op jit(solution)/shard_map/all_gather | solution.py:87
  155.9 0.3 fusion.19
  156.2 0.1 collective-permute-start
  156.3 1.9 collective-permute-done
  158.2 0.1 add.119
  158.3 1.6 collective-permute-start.1
  159.8 12.5 %collective-permute-done.1 = f32[128,1024]{1,0:T(8,128)S(1)} collective-permute-done((f32[128,1024]{1,0:T(8,128)S(1)}, f32[128,1024]{1,0:T(8,128)S(1)}, u32[]{:S(2)}, u32[]{:S(2)}) %collective-permute-start.1) | collective-permute-done | bytes 524320 | tf_op jit(solution)/shard_map/ppermute | solution.py:91
  172.3 0.1 add.120
  172.4 2.5 collective-permute-start.2
  174.8 22.8 %collective-permute-done.2 = f32[128,1024]{1,0:T(8,128)S(1)} collective-permute-done((f32[128,1024]{1,0:T(8,128)S(1)}, f32[128,1024]{1,0:T(8,128)S(1)}, u32[]{:S(2)}, u32[]{:S(2)}) %collective-permute-start.2) | collective-permute-done | bytes 524320 | tf_op jit(solution)/shard_map/ppermute | solution.py:91
  197.7 0.2 multiply_reduce_fusion
  197.8 1.6 convolution_convert_fusion
  199.5 1.6 convolution_convert_fusion.1
  201.1 0.0 reduce-scatter.16.cloned.1.call-start
  201.2 9.0 %psum.30 = f32[128]{0:T(128)S(1)} all-reduce(f32[128]{0:T(128)S(1)} %get-tuple-element.4), channel_id=1, replica_groups=mesh['kv'=4,'tp'=8] {'kv'}, use_global_device_ids=true, to_apply=%region_9.10 | all-reduce | flops 128 | bytes 1024 | tf_op jit(solution)/shard_map/psum | solution.py:22
  210.2 38.4 %all-reduce.3.cloned.1.call-done = (bf16[128,1344]{0,1:T(8,128)(2,1)}, bf16[128,1344]{0,1:T(8,128)(2,1)}) async-done(((bf16[128,1344]{0,1:T(8,128)(2,1)}, bf16[128,1344]{0,1:T(8,128)(2,1)}), (bf16[128,1344]{0,1:T(8,128)(2,1)}, bf16[128,1344]{0,1:T(8,128)(2,1)})) %all-reduce.3.cloned.1.call-update) | async-done | bytes 688144 | tf_op jit(solution)/shard_map/psum | solution.py:25
  248.6 2.8 convolution_convert_fusion.2
  251.4 0.8 copy.18
  252.2 0.0 reduce-scatter.16.cloned.1.call-update
  252.3 31.0 %reduce-scatter.16.cloned.1.call-done = bf16[128,128]{1,0:T(8,128)(2,1)} async-done(((bf16[1024,128]{1,0:T(8,128)(2,1)}), bf16[128,128]{1,0:T(8,128)(2,1)}) %reduce-scatter.16.cloned.1.call-update) | async-done | bytes 32784
  283.2 0.9 copy.19
  284.1 0.6 add_convert_fusion
  (28 shorter events, 0.3 us)
Async XLA Ops:
  7.2 190.7 %copy-start = (bf16[1024,1344]{0,1:T(8,128)(2,1)S(1)}, bf16[1024,1344]{0,1:T(8,128)(2,1)}, u32[]{:S(2)}) copy-start(bf16[1024,1344]{0,1:T(8,128)(2,1)} %param.26) | copy-start | bytes 8257540
  7.2 124.4 %copy-start.5 = (f32[512]{0:T(512)S(1)}, f32[512]{0:T(512)}, u32[]{:S(2)}) copy-start(f32[512]{0:T(512)} %param.20) | copy-start | bytes 6148
  7.2 41.8 %reduce-scatter.10.cloned.1.call-start = ((), (), s32[]{:S(2)}) async-start(), calls=%async_computation.6 | async-start | bytes 327680 | tf_op jit(solution)/shard_map/reduce_scatter | solution.py:67
  24.7 51.5 %reduce-scatter.12.cloned.1.call-start = ((), (), s32[]{:S(2)}) async-start(), calls=%async_computation.7 | async-start | bytes 327680 | tf_op jit(solution)/shard_map/reduce_scatter | solution.py:68
  27.0 76.3 %reduce-scatter.14.cloned.1.call-start = ((), (), s32[]{:S(2)}) async-start(), calls=%async_computation.8 | async-start | bytes 327680 | tf_op jit(solution)/shard_map/reduce_scatter | solution.py:69
  29.3 101.0 %reduce-scatter.8.cloned.1.call-start = ((), (), s32[]{:S(2)}) async-start(), calls=%async_computation.5 | async-start | bytes 327680 | tf_op jit(solution)/shard_map/reduce_scatter | solution.py:66
  31.6 217.0 %all-reduce.3.cloned.1.call-start = ((), (), s32[]{:S(2)}) async-start(), calls=%async_computation.10 | async-start | bytes 1376256 | tf_op jit(solution)/shard_map/psum | solution.py:25
  139.8 59.6 %copy-start.1 = (f32[32,4,128,128]{3,2,1,0:T(8,128)}, f32[32,4,128,128]{3,2,1,0:T(8,128)S(1)}, u32[]{:S(2)}) copy-start(f32[32,4,128,128]{3,2,1,0:T(8,128)S(1)} %multiply_add_fusion) | copy-start | bytes 25165828
  139.8 7.4 %copy-start.6 = (f32[128]{0:T(128)S(1)}, f32[128]{0:T(128)}, u32[]{:S(2)}) copy-start(f32[128]{0:T(128)} %param.22) | copy-start | bytes 1540
  139.9 16.0 %copy-start.3 = (bf16[512,1024]{1,0:T(8,128)(2,1)S(1)}, bf16[512,1024]{1,0:T(8,128)(2,1)}, u32[]{:S(2)}) copy-start(bf16[512,1024]{1,0:T(8,128)(2,1)} %param.23) | copy-start | bytes 3145732
  139.9 58.0 %copy-start.4 = (f32[1024]{0:T(1024)S(1)}, f32[1024]{0:T(1024)}, u32[]{:S(2)}) copy-start(f32[1024]{0:T(1024)} %param.24) | copy-start | bytes 12292
  139.9 59.6 %copy-start.2 = (bf16[1024,1344]{0,1:T(8,128)(2,1)S(1)}, bf16[1024,1344]{0,1:T(8,128)(2,1)}, u32[]{:S(2)}) copy-start(bf16[1024,1344]{0,1:T(8,128)(2,1)} %param.25) | copy-start | bytes 8257540
  156.2 2.0 collective-permute-start
  158.3 14.0 %collective-permute-start.1 = (f32[128,1024]{1,0:T(8,128)S(1)}, f32[128,1024]{1,0:T(8,128)S(1)}, u32[]{:S(2)}, u32[]{:S(2)}) collective-permute-start(f32[128,1024]{1,0:T(8,128)S(1)} %add.119), channel_id=1, source_target_pairs={{0,2},{1,3},{2,0},{3,1},{4,6},{5,7},{6,4},{7,5},{8,10},{9,11},{10,... | collective-permute-start | bytes 1572872 | tf_op jit(solution)/shard_map/ppermute | solution.py:91
  172.4 25.3 %collective-permute-start.2 = (f32[128,1024]{1,0:T(8,128)S(1)}, f32[128,1024]{1,0:T(8,128)S(1)}, u32[]{:S(2)}, u32[]{:S(2)}) collective-permute-start(f32[128,1024]{1,0:T(8,128)S(1)} %add.120), channel_id=1, source_target_pairs={{0,4},{1,5},{2,6},{3,7},{4,0},{5,1},{6,2},{7,3},{8,12},{9,13},{10,... | collective-permute-start | bytes 1572872 | tf_op jit(solution)/shard_map/ppermute | solution.py:91
  201.1 82.1 %reduce-scatter.16.cloned.1.call-start = ((), (), s32[]{:S(2)}) async-start(), calls=%async_computation.9 | async-start | bytes 294912
Sparse Core Ops, SparseCore 0:
  24.8 24.1 reduce-scatter.9
  51.7 24.3 reduce-scatter.11
  78.9 24.3 reduce-scatter.13
  105.9 24.3 reduce-scatter.7
  201.3 47.3 all-reduce.2
  252.4 30.7 reduce-scatter.15
